TPU v7x, 32 devices: a whole 2x2x4 slice. The times are simulated.
32 devices in a mesh: row: 4 (over z), col: 4 (over y, x), dp: 2 (over core).
Axes of the slice: x: 2, y: 2, z: 4, core: 2. Of those that a mesh axis runs over, the one named last changes fastest.
Arguments:
- tokens: bfloat16 [4, 16384, 1024], P('dp', ('row', 'col')), may hold values from -6 to 6
- norm_gain: float32 [1024], replicated, may hold values from 0.5 to 1.5
- in_weight: bfloat16 [1024, 512], replicated, may hold values from -0.1875 to 0.1875
- gate_weight: bfloat16 [1024, 512], replicated, may hold values from -0.1875 to 0.1875
- mix_weight: bfloat16 [512, 512], replicated, may hold values from -0.25 to 0.25
- out_weight: bfloat16 [512, 1024], replicated, may hold values from -0.25 to 0.25
Outputs:
- mixed_out: bfloat16 [4, 16384, 1024], P('dp', ('row', 'col'))
All inputs are finite; a program needn't handle non-finite values.
Results may differ from a plain program's by a relative error of at most 0.007.
Values may be sent and summed in bfloat16 or wider, within the bound.
A program may use at most 128 MiB of HBM per device.

v0:
```python
import jax
import jax.numpy as jnp
import numpy as np
from jax import lax
from jax.sharding import PartitionSpec as P

GROUP_WIDTH = 128
LANES = 128
AXES = ("row", "col")

epsilon = 1e-06
highest = lax.Precision.HIGHEST


def angles(first_len, second_len, period):
    product = np.outer(np.arange(first_len), np.arange(second_len)) % period
    return product * (2.0 * np.pi / period)


def rms_normed(tokens, norm_gain):
    values = tokens.astype(jnp.float32)
    scaled = values * lax.rsqrt(jnp.mean(values * values, axis=-1, keepdims=True) + epsilon)
    return (scaled * norm_gain).astype(jnp.bfloat16)


def packed_in_weight(in_weight):
    model_width, mix_width = in_weight.shape
    phases = angles(GROUP_WIDTH, GROUP_WIDTH, GROUP_WIDTH)
    half = GROUP_WIDTH // 2
    table = np.where(np.arange(GROUP_WIDTH)[None, :] <= half, np.cos(phases), np.sin(phases))
    grouped = in_weight.astype(jnp.float32).reshape(model_width, -1, GROUP_WIDTH)
    packed = jnp.einsum("kgp,pq->kgq", grouped, jnp.asarray(table, jnp.float32), precision=highest)
    return packed.reshape(model_width, mix_width).astype(jnp.bfloat16)


def packed_mix_weight(mix_weight):
    half = GROUP_WIDTH // 2
    table = np.zeros((GROUP_WIDTH, GROUP_WIDTH))
    for q in range(GROUP_WIDTH):
        table[q, q] = 1.0 if q <= half else -1.0
        if q not in (0, half):
            table[q, GROUP_WIDTH - q] = 1.0
    grouped = mix_weight.reshape(-1, GROUP_WIDTH, mix_weight.shape[1])
    packed = jnp.einsum(
        "qr,grm->gqm",
        jnp.asarray(table, jnp.bfloat16),
        grouped,
        preferred_element_type=jnp.float32,
    )
    return packed.reshape(mix_weight.shape).astype(jnp.bfloat16)


def position_transform(arrived, is_sine, norm_scale):
    first_len, seq_count, share, second_len = arrived.shape
    outer = angles(first_len, first_len, first_len)
    outer_table = jnp.asarray(np.stack([np.cos(outer), -np.sin(outer)]), jnp.bfloat16)
    section = jnp.einsum("ran,nscm->rascm", outer_table, arrived, preferred_element_type=jnp.float32)
    twist = angles(first_len, second_len, first_len * second_len)
    twist_cos = jnp.asarray(np.cos(twist), jnp.float32)[:, None, None, :]
    twist_sin = jnp.asarray(np.sin(twist), jnp.float32)[:, None, None, :]
    real = section[0] * twist_cos + section[1] * twist_sin
    imag = section[1] * twist_cos - section[0] * twist_sin
    sine = is_sine[None, None, :, None]
    turned = jnp.stack([jnp.where(sine, -imag, real), jnp.where(sine, real, imag)])
    turned = turned.astype(jnp.bfloat16)
    inner = angles(second_len, second_len, second_len)
    inner_table = jnp.asarray(np.stack([np.cos(inner), np.sin(inner)]), jnp.bfloat16)
    final = jnp.einsum("rbm,rascm->bsca", inner_table, turned, preferred_element_type=jnp.float32)
    return (final * norm_scale).astype(jnp.bfloat16)


def exchange(blocks):
    return lax.all_to_all(blocks, AXES, split_axis=0, concat_axis=0, tiled=True)


def body(tokens, norm_gain, in_weight, gate_weight, mix_weight, out_weight):
    seq_count, positions, model_width = tokens.shape
    mix_width = in_weight.shape[1]
    pieces = lax.axis_size(AXES)
    length = positions * pieces
    share = mix_width // pieces
    tiles = positions // LANES
    norm_scale = (length * GROUP_WIDTH) ** (-0.5)
    normed = rms_normed(tokens, norm_gain).reshape(seq_count * positions, model_width)
    packed = lax.dot_general(
        packed_in_weight(in_weight),
        normed,
        (((0,), (1,)), ((), ())),
        preferred_element_type=jnp.float32,
    ).astype(jnp.bfloat16)
    packed = packed.reshape(pieces, share, seq_count, tiles, LANES).transpose(0, 3, 2, 1, 4)
    arrived = exchange(packed)
    gate_values = jnp.dot(normed, gate_weight, preferred_element_type=jnp.float32).astype(
        jnp.bfloat16
    )
    arrived = arrived.reshape(pieces * tiles, seq_count, share, LANES)
    column = lax.axis_index(AXES) * share + jnp.arange(share)
    is_sine = column % GROUP_WIDTH > GROUP_WIDTH // 2
    send_back = position_transform(arrived, is_sine, norm_scale)
    high_count = send_back.shape[0] // pieces
    low_count = send_back.shape[-1]
    send_back = send_back.reshape(pieces, high_count, seq_count, share, low_count)
    returned = exchange(send_back)
    mix_rows = packed_mix_weight(mix_weight).reshape(pieces, share, mix_width)
    mixed = jnp.einsum(
        "dbsca,dcm->sbam", returned, mix_rows, preferred_element_type=jnp.float32
    ).reshape(seq_count * positions, mix_width)
    gated_out = (mixed * jax.nn.silu(gate_values.astype(jnp.float32))).astype(jnp.bfloat16)
    output = jnp.dot(gated_out, out_weight, preferred_element_type=jnp.float32).astype(jnp.bfloat16)
    return output.reshape(seq_count, positions, model_width)


def solution(mesh):
    return jax.shard_map(
        body,
        mesh=mesh,
        in_specs=(P("dp", AXES, None), P(), P(), P(), P(), P()),
        out_specs=P("dp", AXES, None),
        check_vma=False,
    )
```

profile of v0, /device:TPU:12, one launch (start us, length us, event | category | flops | bytes accessed | tf_op | source)
XLA Modules:
  0.0 138.4 jit_solution(12619161370745945649)
XLA Ops:
  0.0 0.0 copy-start
  0.0 0.0 copy-start.1
  0.0 0.0 copy-start.11
  0.0 3.2 %fusion = f32[2,1024]{1,0:T(2,128)S(1)} fusion(bf16[2,1024,1024]{2,1,0:T(8,128)(2,1)} %param.12), kind=kLoop, calls=%fused_computation.2 | loop fusion | flops 6289408 | bytes 4202496 | tf_op jit(solution)/shard_map/reduce_sum | solution.py:22
  3.3 0.3 copy-done.1
  3.5 0.0 copy-done.11
  3.5 0.0 copy-start.4
  3.5 0.0 copy-start.9
  3.5 1.1 fusion.2
  4.7 0.1 copy-done.4
  4.8 0.0 copy-done.9
  4.8 0.0 copy-start.2
  4.8 1.0 convolution_convert_fusion.3
  5.8 2.4 %fusion.17 = bf16[64,8,16,128]{3,1,2,0:T(8,128)(2,1)S(1)} fusion(bf16[1024,512]{0,1:T(8,128)(2,1)S(1)} %bitcast.79, bf16[2048,1024]{1,0:T(8,128)(2,1)S(1)} %bitcast.76), kind=kOutput, calls=%fused_computation.30 | convolution fusion | flops 2148532224 | bytes 7340032 | tf_op jit(solution)/shard_map/dot_general | solution.py:85
  8.2 0.0 copy-done.2
  8.2 0.0 copy-start.8
  8.2 2.0 %copy.35 = bf16[64,8,16,128]{3,2,1,0:T(8,128)(2,1)} copy(bf16[64,8,16,128]{3,1,2,0:T(8,128)(2,1)S(1)} %fusion.17) | data formatting | bytes 4194304
  10.2 7.2 %all-to-all-start = ((bf16[16,8,2,32,128]{4,1,2,3,0:T(8,128)(2,1)}), bf16[16,8,2,32,128]{4,1,2,3,0:T(8,128)(2,1)S(1)}, u32[]{:S(2)}, u32[]{:S(2)}) async-start(bf16[16,8,2,32,128]{4,1,2,3,0:T(8,128)(2,1)} %bitcast.75), calls=%async_computation | async-start | bytes 4194304 | tf_op jit(solution)/shard_map/all_to_all | solution.py:73
  17.3 0.0 copy-start.6
  17.3 0.0 copy-start.7
  17.4 48.4 %all-to-all-done = bf16[16,8,2,32,128]{4,1,2,3,0:T(8,128)(2,1)S(1)} async-done(((bf16[16,8,2,32,128]{4,1,2,3,0:T(8,128)(2,1)}), bf16[16,8,2,32,128]{4,1,2,3,0:T(8,128)(2,1)S(1)}, u32[]{:S(2)}, u32[]{:S(2)}) %all-to-all-start) | async-done | bytes 2097184 | tf_op jit(solution)/shard_map/all_to_all | solution.py:73
  65.7 0.0 copy-done.8
  65.8 1.2 fusion.14
  67.0 0.0 copy-done.6
  67.0 0.0 copy-done.7
  67.0 0.0 copy-start.5
  67.0 1.7 %select_convert_fusion.1 = (bf16[1,128,2,32,128]{4,1,3,2,0:T(8,128)(2,1)S(1)}, bf16[1,128,2,32,128]{4,1,3,2,0:T(8,128)(2,1)S(1)}) fusion(pred[32]{0:T(512)(128)(4,1)S(1)} %fusion.20, f32[128,128]{1,0:T(8,128)S(1)} %copy-done.7, f32[2,128,2,32,128]{4,1,3,2,0:T(8,128)S(1)} %fusion.14, f32[128,128]{1,0:T(8,128)S(1)} %copy-done.6), kind=kLoop, calls=%fused_computation.18 | loop fusion | flops 11534336 | bytes 12714016 | tf_op jit(solution)/shard_map/convert
  68.7 0.0 copy-done.5
  68.7 1.5 %fusion.7 = f32[128,2,32,128,1]{0,3,2,1,4:T(8,128)S(1)} fusion(bf16[2,128,128,1,1]{2,1,4,3,0:T(8,128)(2,1)S(1)} %copy-done.5, bf16[1,128,2,32,128]{4,1,3,2,0:T(8,128)(2,1)S(1)} %get-tuple-element.6, bf16[1,128,2,32,128]{4,1,3,2,0:T(8,128)(2,1)S(1)} %get-tuple-element.5), kind=kOutput, calls=%fused_computation.11 | convolution fusion | flops 538968064 | bytes 8454144 | tf_op jit(solution)/shard_map/rbm,rascm->bsca/dot_general | solution.py:68
  70.2 0.6 fusion.13
  70.8 0.0 copy-start.10
  70.9 2.7 %copy.25 = bf16[16,8,2,32,128]{4,3,2,1,0:T(8,128)(2,1)} copy(bf16[16,8,2,32,128]{4,1,0,2,3:T(8,128)(2,1)S(1)} %fusion.13) | data formatting | bytes 4194304 | tf_op jit(solution)/shard_map/reshape | solution.py:102
  73.5 5.6 %all-to-all-start.1 = ((bf16[16,8,2,32,128]{4,3,2,1,0:T(8,128)(2,1)}), bf16[16,8,2,32,128]{4,3,2,1,0:T(8,128)(2,1)S(1)}, u32[]{:S(2)}, u32[]{:S(2)}) async-start(bf16[16,8,2,32,128]{4,3,2,1,0:T(8,128)(2,1)} %copy.25), calls=%async_computation.1 | async-start | bytes 4194304 | tf_op jit(solution)/shard_map/all_to_all | solution.py:73
  79.1 0.0 copy-done.10
  79.1 2.1 %convolution_convert_fusion.4 = bf16[128,4,512]{2,0,1:T(8,128)(2,1)} fusion(bf16[128,128,1]{1,0,2:T(8,128)(2,1)S(1)} %copy-done.10, bf16[4,128,512]{2,1,0:T(8,128)(2,1)} %bitcast.80), kind=kOutput, calls=%fused_computation.32 | convolution fusion | flops 67371008 | bytes 1081344 | tf_op jit(solution)/shard_map/qr,grm->gqm/dot_general | solution.py:44
  81.3 44.8 %all-to-all-done.1 = bf16[16,8,2,32,128]{4,3,2,1,0:T(8,128)(2,1)S(1)} async-done(((bf16[16,8,2,32,128]{4,3,2,1,0:T(8,128)(2,1)}), bf16[16,8,2,32,128]{4,3,2,1,0:T(8,128)(2,1)S(1)}, u32[]{:S(2)}, u32[]{:S(2)}) %all-to-all-start.1) | async-done | bytes 2097184 | tf_op jit(solution)/shard_map/all_to_all | solution.py:73
  126.1 2.3 %convolution_bitcast_fusion = f32[2,8,128,512]{3,2,0,1:T(8,128)S(1)} fusion(bf16[16,32,512,1,1]{2,1,4,3,0:T(8,128)(2,1)} %bitcast.78, bf16[16,8,2,32,128]{4,3,2,1,0:T(8,128)(2,1)S(1)} %all-to-all-done.1), kind=kOutput, calls=%fused_computation.25 | convolution fusion | flops 1073741824 | bytes 6815744 | tf_op jit(solution)/shard_map/dbsca,dcm->sbam/dot_general | solution.py:105
  128.4 0.0 copy-start.3
  128.4 0.0 copy-start.12
  128.4 0.6 copy.27
  129.0 1.6 %copy-done.3 = bf16[2,1024,1024]{2,1,0:T(8,128)(2,1)S(1)} copy-done((bf16[2,1024,1024]{2,1,0:T(8,128)(2,1)S(1)}, bf16[2,1024,1024]{2,1,0:T(8,128)(2,1)}, u32[]{:S(2)}) %copy-start.3) | copy-done | bytes 4194328
  130.6 0.3 copy-done.12
  130.9 3.1 %fusion.12 = bf16[2048,512]{1,0:T(8,128)(2,1)S(1)} fusion(f32[2,8,128,512]{3,2,1,0:T(8,128)S(1)} %copy.27, bf16[2048,1024]{1,0:T(8,128)(2,1)S(1)} %bitcast.77, bf16[1024,512]{1,0:T(8,128)(2,1)S(1)} %copy-done.12), kind=kOutput, calls=%fused_computation.21 | convolution fusion | flops 2155872256 | bytes 11534336 | tf_op jit(solution)/shard_map/dot_general | solution.py:93
  134.0 0.0 copy-done
  134.0 4.4 %convolution_convert_fusion = bf16[2048,1024]{1,0:T(8,128)(2,1)} fusion(bf16[2048,512]{1,0:T(8,128)(2,1)S(1)} %fusion.12, bf16[512,1024]{1,0:T(8,128)(2,1)S(1)} %copy-done), kind=kOutput, calls=%fused_computation.22 | convolution fusion | flops 2149580800 | bytes 7340032 | tf_op jit(solution)/shard_map/dot_general | solution.py:109
  (2 shorter events, 0.0 us)
Async XLA Ops:
  0.0 134.0 %copy-start = (bf16[512,1024]{1,0:T(8,128)(2,1)S(1)}, bf16[512,1024]{1,0:T(8,128)(2,1)}, u32[]{:S(2)}) copy-start(bf16[512,1024]{1,0:T(8,128)(2,1)} %param.17) | copy-start | bytes 3145732
  0.0 3.5 %copy-start.1 = (bf16[2,1024,1024]{2,1,0:T(8,128)(2,1)S(1)}, bf16[2,1024,1024]{2,1,0:T(8,128)(2,1)}, u32[]{:S(2)}) copy-start(bf16[2,1024,1024]{2,1,0:T(8,128)(2,1)} %param.12) | copy-start | bytes 12582916
  0.0 3.5 %copy-start.11 = (f32[1024]{0:T(1024)S(1)}, f32[1024]{0:T(1024)}, u32[]{:S(2)}) copy-start(f32[1024]{0:T(1024)} %param.13) | copy-start | bytes 12292
  3.5 1.2 copy-start.4
  3.5 1.2 copy-start.9
  4.8 3.4 %copy-start.2 = (bf16[2,1024,1024]{2,1,0:T(8,128)(2,1)}, bf16[2,1024,1024]{2,1,0:T(8,128)(2,1)S(1)}, u32[]{:S(2)}) copy-start(bf16[2,1024,1024]{2,1,0:T(8,128)(2,1)S(1)} %fusion.2) | copy-start | bytes 12582916
  8.2 57.6 %copy-start.8 = (bf16[2,128,128,1,1]{2,1,4,3,0:T(8,128)(2,1)S(1)}, bf16[2,128,128,1,1]{2,1,4,3,0:T(8,128)(2,1)}, u32[]{:S(2)}) copy-start(bf16[2,128,128,1,1]{2,1,4,3,0:T(8,128)(2,1)} %constant.61) | copy-start | bytes 196612
  10.2 55.6 %all-to-all-start = ((bf16[16,8,2,32,128]{4,1,2,3,0:T(8,128)(2,1)}), bf16[16,8,2,32,128]{4,1,2,3,0:T(8,128)(2,1)S(1)}, u32[]{:S(2)}, u32[]{:S(2)}) async-start(bf16[16,8,2,32,128]{4,1,2,3,0:T(8,128)(2,1)} %bitcast.75), calls=%async_computation | async-start | bytes 4194304 | tf_op jit(solution)/shard_map/all_to_all | solution.py:73
  17.3 49.7 %copy-start.6 = (f32[128,128]{1,0:T(8,128)S(1)}, f32[128,128]{1,0:T(8,128)}, u32[]{:S(2)}) copy-start(f32[128,128]{1,0:T(8,128)} %constant.56.clone) | copy-start | bytes 196612
  17.3 49.7 %copy-start.7 = (f32[128,128]{1,0:T(8,128)S(1)}, f32[128,128]{1,0:T(8,128)}, u32[]{:S(2)}) copy-start(f32[128,128]{1,0:T(8,128)} %constant.57.clone) | copy-start | bytes 196612
  67.0 1.7 %copy-start.5 = (bf16[2,128,128,1,1]{2,1,4,3,0:T(8,128)(2,1)S(1)}, bf16[2,128,128,1,1]{2,1,4,3,0:T(8,128)(2,1)}, u32[]{:S(2)}) copy-start(bf16[2,128,128,1,1]{2,1,4,3,0:T(8,128)(2,1)} %constant.63) | copy-start | bytes 196612
  70.8 8.3 %copy-start.10 = (bf16[128,128,1]{1,0,2:T(8,128)(2,1)S(1)}, bf16[128,128,1]{1,0,2:T(8,128)(2,1)}, u32[]{:S(2)}) copy-start(bf16[128,128,1]{1,0,2:T(8,128)(2,1)} %constant.60) | copy-start | bytes 98308
  73.5 52.5 %all-to-all-start.1 = ((bf16[16,8,2,32,128]{4,3,2,1,0:T(8,128)(2,1)}), bf16[16,8,2,32,128]{4,3,2,1,0:T(8,128)(2,1)S(1)}, u32[]{:S(2)}, u32[]{:S(2)}) async-start(bf16[16,8,2,32,128]{4,3,2,1,0:T(8,128)(2,1)} %copy.25), calls=%async_computation.1 | async-start | bytes 4194304 | tf_op jit(solution)/shard_map/all_to_all | solution.py:73
  128.4 2.2 %copy-start.3 = (bf16[2,1024,1024]{2,1,0:T(8,128)(2,1)S(1)}, bf16[2,1024,1024]{2,1,0:T(8,128)(2,1)}, u32[]{:S(2)}) copy-start(bf16[2,1024,1024]{2,1,0:T(8,128)(2,1)} %copy-done.2) | copy-start | bytes 12582916
  128.4 2.5 %copy-start.12 = (bf16[1024,512]{1,0:T(8,128)(2,1)S(1)}, bf16[1024,512]{1,0:T(8,128)(2,1)}, u32[]{:S(2)}) copy-start(bf16[1024,512]{1,0:T(8,128)(2,1)} %param.15) | copy-start | bytes 3145732
where the time goes:
time: 139 us; the launch traced here: 138 us
  waiting for transfers between devices  93.2 us (67%)
  matrix products  18 us (13%)
  starting transfers between devices  12.7 us (9%)
  local copies, waits for them, and re-layouts  7.56 us (5%)
  other arithmetic  6.66 us (5%)
    all_to_all x2, waiting for transfers between devices, exchange(): return lax.all_to_all(blocks, AXES, split_axis=0, concat_axis=0, tiled=True)  93.2 us
    all_to_all x2, starting transfers between devices, exchange(): return lax.all_to_all(blocks, AXES, split_axis=0, concat_axis=0, tiled=True)  12.7 us
    dot_general x1, matrix products, body(): jnp.dot(gated_out, out_weight, preferred_element_type=jnp.float32)  4.36 us
    unnamed x27, local copies, waits for them, and re-layouts  4.28 us
    reduce_sum x1, other arithmetic, rms_normed(): jnp.mean(values * values, axis=-1, keepdims=True) + epsilon  3.23 us
    dot_general x1, matrix products, body(): jnp.dot(normed, gate_weight, preferred_element_type=jnp.float32)  3.09 us
  transfers between devices with their start and end apart: 2, of which 2 were waited for; matrix products, arithmetic and copies ran while one was open for 2% of the time, Pallas kernels for 0%

commit v1 on v0

--- a/solution.py
+++ b/solution.py
@@ -1,7 +1,11 @@
+import functools
+
 import jax
 import jax.numpy as jnp
 import numpy as np
 from jax import lax
+from jax.experimental import pallas as pl
+from jax.experimental.pallas import tpu as pltpu
 from jax.sharding import PartitionSpec as P
 
 GROUP_WIDTH = 128
@@ -69,8 +73,53 @@
     return (final * norm_scale).astype(jnp.bfloat16)
 
 
-def exchange(blocks):
-    return lax.all_to_all(blocks, AXES, split_axis=0, concat_axis=0, tiled=True)
+def exchange_kernel(pieces, col_count, sent_ref, out_ref, send_sems, recv_sems, own_sem):
+    me = lax.axis_index("row") * col_count + lax.axis_index("col")
+
+    def place(step):
+        peer = lax.rem(me + step, pieces)
+        return peer, {"row": peer // col_count, "col": peer % col_count}
+
+    barrier = pltpu.get_barrier_semaphore()
+    for step in range(1, pieces):
+        pl.semaphore_signal(
+            barrier, inc=1, device_id=place(step)[1], device_id_type=pl.DeviceIdType.MESH
+        )
+    pl.semaphore_wait(barrier, pieces - 1)
+    copies = []
+    for step in range(1, pieces):
+        peer, where = place(step)
+        copy = pltpu.make_async_remote_copy(
+            src_ref=sent_ref.at[peer],
+            dst_ref=out_ref.at[me],
+            send_sem=send_sems.at[step],
+            recv_sem=recv_sems.at[step],
+            device_id=where,
+            device_id_type=pl.DeviceIdType.MESH,
+        )
+        copy.start()
+        copies.append(copy)
+    own = pltpu.make_async_copy(sent_ref.at[me], out_ref.at[me], own_sem)
+    own.start()
+    own.wait()
+    for copy in copies:
+        copy.wait()
+
+
+def exchange(blocks, call_id):
+    pieces = blocks.shape[0]
+    return pl.pallas_call(
+        functools.partial(exchange_kernel, pieces, lax.axis_size("col")),
+        out_shape=jax.ShapeDtypeStruct(blocks.shape, blocks.dtype),
+        in_specs=[pl.BlockSpec(memory_space=pltpu.VMEM)],
+        out_specs=pl.BlockSpec(memory_space=pltpu.VMEM),
+        scratch_shapes=[
+            pltpu.SemaphoreType.DMA((pieces,)),
+            pltpu.SemaphoreType.DMA((pieces,)),
+            pltpu.SemaphoreType.DMA,
+        ],
+        compiler_params=pltpu.CompilerParams(collective_id=call_id, has_side_effects=True),
+    )(blocks)
 
 
 def body(tokens, norm_gain, in_weight, gate_weight, mix_weight, out_weight):
@@ -89,7 +138,7 @@
         preferred_element_type=jnp.float32,
     ).astype(jnp.bfloat16)
     packed = packed.reshape(pieces, share, seq_count, tiles, LANES).transpose(0, 3, 2, 1, 4)
-    arrived = exchange(packed)
+    arrived = exchange(packed, 0)
     gate_values = jnp.dot(normed, gate_weight, preferred_element_type=jnp.float32).astype(
         jnp.bfloat16
     )
@@ -100,7 +149,7 @@
     high_count = send_back.shape[0] // pieces
     low_count = send_back.shape[-1]
     send_back = send_back.reshape(pieces, high_count, seq_count, share, low_count)
-    returned = exchange(send_back)
+    returned = exchange(send_back, 1)
     mix_rows = packed_mix_weight(mix_weight).reshape(pieces, share, mix_width)
     mixed = jnp.einsum(
         "dbsca,dcm->sbam", returned, mix_rows, preferred_element_type=jnp.float32

time: 139 us -> 145 us (1.043)
  Pallas kernels: 0 us -> 109 us
  waiting for transfers between devices: 93.2 us -> 0 us
  starting transfers between devices: 12.7 us -> 0 us
    pallas_call x0 -> x2, Pallas kernels: none -> 109 us  [exchange(): pl.pallas_call(functools.partial(exchange_kernel, pieces, lax.axis_size('...]
    all_to_all x2 -> x0, waiting for transfers between devices: 93.2 us -> none  [exchange(): return lax.all_to_all(blocks, AXES, split_axis=0, concat_axis=0, tiled=True)]
    all_to_all x2 -> x0, starting transfers between devices: 12.7 us -> none  [exchange(): return lax.all_to_all(blocks, AXES, split_axis=0, concat_axis=0, tiled=True)]
    convert_element_type x0 -> x1, local copies, waits for them, and re-layouts: none -> 2.68 us  [position_transform(): return (final * norm_scale).astype(jnp.bfloat16)]
    dot_general x1, matrix products: 1.24 us -> 3.43 us  [position_transform(): jnp.einsum('ran,nscm->rascm', outer_table, arrived, preferred_element_typ...]
    dot_general x1, matrix products: 2.14 us -> 0.28 us  [packed_mix_weight(): jnp.einsum('qr,grm->gqm', jnp.asarray(table, jnp.bfloat16), grouped, pref...]
    unnamed x27 -> x29, local copies, waits for them, and re-layouts: 4.28 us -> 2.9 us
  transfers between devices with their start and end apart: 2 -> 0, of which waited for: 2 -> 0; matrix products, arithmetic and copies ran while one was open for 2% -> 0% of each run, Pallas kernels for 0% -> 0%
where the time goes in v1:
time: 145 us; the launch traced here: 143 us
  Pallas kernels  109 us (75%)
  matrix products  19.1 us (13%)
  local copies, waits for them, and re-layouts  8.08 us (6%)
  other arithmetic  6.67 us (5%)
    pallas_call x2, Pallas kernels, exchange(): pl.pallas_call(functools.partial(exchange_kernel, pieces, lax.axis_size('...  109 us
    dot_general x1, matrix products, body(): jnp.dot(gated_out, out_weight, preferred_element_type=jnp.float32)  4.36 us
    dot_general x1, matrix products, position_transform(): jnp.einsum('ran,nscm->rascm', outer_table, arrived, preferred_element_typ...  3.43 us
    reduce_sum x1, other arithmetic, rms_normed(): jnp.mean(values * values, axis=-1, keepdims=True) + epsilon  3.23 us
    dot_general x1, matrix products, body(): jnp.dot(normed, gate_weight, preferred_element_type=jnp.float32)  3.09 us
    unnamed x29, local copies, waits for them, and re-layouts  2.9 us

profile of v1, /device:TPU:12, one launch (start us, length us, event | category | flops | bytes accessed | tf_op | source)
XLA Modules:
  0.0 143.0 jit_solution(11519309337425773066)
XLA Ops:
  0.0 0.0 copy-start
  0.0 0.0 copy-start.11
  0.0 0.0 copy-start.1
  0.0 3.2 %fusion = f32[2,1024]{1,0:T(2,128)S(1)} fusion(bf16[2,1024,1024]{2,1,0:T(8,128)(2,1)} %param.12), kind=kLoop, calls=%fused_computation.2 | loop fusion | flops 6289408 | bytes 4202496 | tf_op jit(solution)/shard_map/reduce_sum | solution.py:26
  3.3 0.0 copy-done.11
  3.3 0.3 copy-done.1
  3.6 0.0 copy-start.4
  3.6 0.0 copy-start.9
  3.6 1.1 fusion.2
  4.7 0.0 copy-start.2
  4.7 0.1 copy-done.4
  4.8 0.0 copy-done.9
  4.8 1.0 convolution_convert_fusion.3
  5.8 2.4 %fusion.15 = bf16[64,8,16,128]{3,1,2,0:T(8,128)(2,1)S(1)} fusion(bf16[1024,512]{0,1:T(8,128)(2,1)S(1)} %bitcast.81, bf16[2048,1024]{1,0:T(8,128)(2,1)S(1)} %bitcast.78), kind=kOutput, calls=%fused_computation.30 | convolution fusion | flops 2148532224 | bytes 7340032 | tf_op jit(solution)/shard_map/dot_general | solution.py:134
  8.2 0.0 copy-done.2
  8.2 0.6 copy.33
  8.8 0.0 copy-start.8
  8.8 1.9 %copy.48 = bf16[16,32,2,8,128]{4,1,2,3,0:T(8,128)(2,1)} copy(bf16[16,32,2,8,128]{4,3,2,1,0:T(8,128)(2,1)S(1)} %bitcast.75) | data formatting | bytes 4194304 | tf_op jit(solution)/shard_map/reshape | solution.py:140
  10.7 55.5 %shard_map.118 = bf16[16,8,2,32,128]{4,3,2,1,0:T(8,128)(2,1)} custom-call(bf16[16,8,2,32,128]{4,3,2,1,0:T(8,128)(2,1)} %bitcast.76), custom_call_target="tpu_custom_call" | custom-call | tf_op jit(solution)/shard_map/pallas_call | solution.py:111
  66.2 0.0 copy-done.8
  66.2 0.0 copy-start.6
  66.2 0.0 copy-start.7
  66.2 3.4 %fusion.12 = f32[2,128,2,32,128]{4,1,3,2,0:T(8,128)S(1)} fusion(bf16[2,128,128,1,1]{2,1,4,3,0:T(8,128)(2,1)S(1)} %copy-done.8, bf16[128,2,32,128]{3,2,1,0:T(8,128)(2,1)} %bitcast.74), kind=kOutput, calls=%fused_computation.26 | convolution fusion | flops 536870912 | bytes 10551296 | tf_op jit(solution)/shard_map/ran,nscm->rascm/dot_general | solution.py:61
  69.7 0.0 copy-done.6
  69.7 0.0 copy-done.7
  69.7 0.0 copy-start.13
  69.7 1.7 %select_convert_fusion.1 = (bf16[1,128,2,32,128]{4,1,3,2,0:T(8,128)(2,1)S(1)}, bf16[1,128,2,32,128]{4,1,3,2,0:T(8,128)(2,1)S(1)}) fusion(pred[32]{0:T(512)(128)(4,1)S(1)} %fusion.18, f32[128,128]{1,0:T(8,128)S(1)} %copy-done.7, f32[2,128,2,32,128]{4,1,3,2,0:T(8,128)S(1)} %fusion.12, f32[128,128]{1,0:T(8,128)S(1)} %copy-done.6), kind=kLoop, calls=%fused_computation.17 | loop fusion | flops 11534336 | bytes 12714016 | tf_op jit(solution)/shard_map/convert
  71.4 0.0 copy-done.13
  71.4 1.7 %fusion.8 = f32[128,2,32,128,1]{0,3,1,2,4:T(8,128)S(1)} fusion(bf16[2,128,128,1,1]{2,1,3,4,0:T(8,128)(2,1)S(1)} %copy-done.13, bf16[1,128,2,32,128]{4,1,3,2,0:T(8,128)(2,1)S(1)} %get-tuple-element.6, bf16[1,128,2,32,128]{4,1,3,2,0:T(8,128)(2,1)S(1)} %get-tuple-element.5), kind=kOutput, calls=%fused_computation.14 | convolution fusion | flops 538968064 | bytes 8454144 | tf_op jit(solution)/shard_map/rbm,rascm->bsca/dot_general | solution.py:72
  73.1 0.6 fusion.11
  73.7 0.0 copy-start.5
  73.7 0.0 copy-start.10
  73.7 2.7 %copy.22 = bf16[128,2,32,128]{3,2,1,0:T(8,128)(2,1)} copy(bf16[128,2,32,128]{3,0,2,1:T(8,128)(2,1)S(1)} %fusion.11) | data formatting | bytes 4194304 | tf_op jit(solution)/shard_map/convert_element_type | solution.py:73
  76.4 53.5 %shard_map.119 = bf16[16,8,2,32,128]{4,3,2,1,0:T(8,128)(2,1)} custom-call(bf16[16,8,2,32,128]{4,3,2,1,0:T(8,128)(2,1)} %bitcast.77), custom_call_target="tpu_custom_call" | custom-call | tf_op jit(solution)/shard_map/pallas_call | solution.py:111
  129.9 0.0 copy-done.5
  129.9 0.0 copy-done.10
  129.9 0.3 convolution_convert_fusion.4
  130.2 2.9 %convolution_bitcast_fusion = f32[2,8,128,512]{3,2,0,1:T(8,128)S(1)} fusion(bf16[16,32,512,1,1]{2,1,4,3,0:T(8,128)(2,1)S(1)} %bitcast.80, bf16[16,8,2,32,128]{4,3,2,1,0:T(8,128)(2,1)} %shard_map.119), kind=kOutput, calls=%fused_computation.24 | convolution fusion | flops 1073741824 | bytes 6815744 | tf_op jit(solution)/shard_map/dbsca,dcm->sbam/dot_general | solution.py:154
  133.1 0.0 copy-start.3
  133.1 0.0 copy-start.12
  133.1 0.6 copy.24
  133.7 1.6 %copy-done.3 = bf16[2,1024,1024]{2,1,0:T(8,128)(2,1)S(1)} copy-done((bf16[2,1024,1024]{2,1,0:T(8,128)(2,1)S(1)}, bf16[2,1024,1024]{2,1,0:T(8,128)(2,1)}, u32[]{:S(2)}) %copy-start.3) | copy-done | bytes 4194328
  135.3 0.3 copy-done.12
  135.6 3.1 %fusion.10 = bf16[2048,512]{1,0:T(8,128)(2,1)S(1)} fusion(f32[2,8,128,512]{3,2,1,0:T(8,128)S(1)} %copy.24, bf16[2048,1024]{1,0:T(8,128)(2,1)S(1)} %bitcast.79, bf16[1024,512]{1,0:T(8,128)(2,1)S(1)} %copy-done.12), kind=kOutput, calls=%fused_computation.20 | convolution fusion | flops 2155872256 | bytes 11534336 | tf_op jit(solution)/shard_map/dot_general | solution.py:142
  138.7 0.0 copy-done
  138.7 4.4 %convolution_convert_fusion = bf16[2048,1024]{1,0:T(8,128)(2,1)} fusion(bf16[2048,512]{1,0:T(8,128)(2,1)S(1)} %fusion.10, bf16[512,1024]{1,0:T(8,128)(2,1)S(1)} %copy-done), kind=kOutput, calls=%fused_computation.21 | convolution fusion | flops 2149580800 | bytes 7340032 | tf_op jit(solution)/shard_map/dot_general | solution.py:158
  (2 shorter events, 0.0 us)
Async XLA Ops:
  0.0 138.7 %copy-start = (bf16[512,1024]{1,0:T(8,128)(2,1)S(1)}, bf16[512,1024]{1,0:T(8,128)(2,1)}, u32[]{:S(2)}) copy-start(bf16[512,1024]{1,0:T(8,128)(2,1)} %param.17) | copy-start | bytes 3145732
  0.0 3.3 %copy-start.11 = (f32[1024]{0:T(1024)S(1)}, f32[1024]{0:T(1024)}, u32[]{:S(2)}) copy-start(f32[1024]{0:T(1024)} %param.13) | copy-start | bytes 12292
  0.0 3.6 %copy-start.1 = (bf16[2,1024,1024]{2,1,0:T(8,128)(2,1)S(1)}, bf16[2,1024,1024]{2,1,0:T(8,128)(2,1)}, u32[]{:S(2)}) copy-start(bf16[2,1024,1024]{2,1,0:T(8,128)(2,1)} %param.12) | copy-start | bytes 12582916
  3.6 1.2 copy-start.4
  3.6 1.2 copy-start.9
  4.7 3.5 %copy-start.2 = (bf16[2,1024,1024]{2,1,0:T(8,128)(2,1)}, bf16[2,1024,1024]{2,1,0:T(8,128)(2,1)S(1)}, u32[]{:S(2)}) copy-start(bf16[2,1024,1024]{2,1,0:T(8,128)(2,1)S(1)} %fusion.2) | copy-start | bytes 12582916
  8.8 57.4 %copy-start.8 = (bf16[2,128,128,1,1]{2,1,4,3,0:T(8,128)(2,1)S(1)}, bf16[2,128,128,1,1]{2,1,4,3,0:T(8,128)(2,1)}, u32[]{:S(2)}) copy-start(bf16[2,128,128,1,1]{2,1,4,3,0:T(8,128)(2,1)} %constant.61) | copy-start | bytes 196612
  66.2 3.5 %copy-start.6 = (f32[128,128]{1,0:T(8,128)S(1)}, f32[128,128]{1,0:T(8,128)}, u32[]{:S(2)}) copy-start(f32[128,128]{1,0:T(8,128)} %constant.56.clone) | copy-start | bytes 196612
  66.2 3.5 %copy-start.7 = (f32[128,128]{1,0:T(8,128)S(1)}, f32[128,128]{1,0:T(8,128)}, u32[]{:S(2)}) copy-start(f32[128,128]{1,0:T(8,128)} %constant.57.clone) | copy-start | bytes 196612
  69.7 1.7 %copy-start.13 = (bf16[2,128,128,1,1]{2,1,3,4,0:T(8,128)(2,1)S(1)}, bf16[2,128,128,1,1]{2,1,3,4,0:T(8,128)(2,1)}, u32[]{:S(2)}) copy-start(bf16[2,128,128,1,1]{2,1,3,4,0:T(8,128)(2,1)} %constant.63) | copy-start | bytes 196612
  73.7 56.2 %copy-start.5 = (bf16[512,512]{1,0:T(8,128)(2,1)S(1)}, bf16[512,512]{1,0:T(8,128)(2,1)}, u32[]{:S(2)}) copy-start(bf16[512,512]{1,0:T(8,128)(2,1)} %param.16) | copy-start | bytes 1572868
  73.7 56.2 %copy-start.10 = (bf16[128,128,1]{1,0,2:T(8,128)(2,1)S(1)}, bf16[128,128,1]{1,0,2:T(8,128)(2,1)}, u32[]{:S(2)}) copy-start(bf16[128,128,1]{1,0,2:T(8,128)(2,1)} %constant.60) | copy-start | bytes 98308
  133.1 2.2 %copy-start.3 = (bf16[2,1024,1024]{2,1,0:T(8,128)(2,1)S(1)}, bf16[2,1024,1024]{2,1,0:T(8,128)(2,1)}, u32[]{:S(2)}) copy-start(bf16[2,1024,1024]{2,1,0:T(8,128)(2,1)} %copy-done.2) | copy-start | bytes 12582916
  133.1 2.5 %copy-start.12 = (bf16[1024,512]{1,0:T(8,128)(2,1)S(1)}, bf16[1024,512]{1,0:T(8,128)(2,1)}, u32[]{:S(2)}) copy-start(bf16[1024,512]{1,0:T(8,128)(2,1)} %param.15) | copy-start | bytes 3145732
